TPU v7x, 256 devices: a whole 4x4x8 slice. The times are simulated.
256 devices in a mesh: sp: 32 (over z, x), tp: 4 (over y), dp: 2 (over core).
Axes of the slice: x: 4, y: 4, z: 8, core: 2. Of those that a mesh axis runs over, the one named last changes fastest.
Arguments:
- latent: bfloat16 [2, 16384, 2048], P('dp', ('sp', 'tp')), may hold values from -6 to 6
- condition: float32 [2, 2048], P('dp'), may hold values from -6 to 6
- context: bfloat16 [2, 1024, 2048], P('dp', 'sp'), may hold values from -6 to 6
- context_cond: float32 [2048], replicated, may hold values from -6 to 6
- shift_matrix: bfloat16 [2048, 2048], P(('sp', 'tp')), may hold values from -0.125 to 0.125
- scale_matrix: bfloat16 [2048, 2048], P(('sp', 'tp')), may hold values from -0.125 to 0.125
- gate_matrix: bfloat16 [2048, 2048], P(('sp', 'tp')), may hold values from -0.125 to 0.125
- value_proj: bfloat16 [2048, 2048], P(None, 'tp'), may hold values from -0.125 to 0.125
- gate_proj: bfloat16 [2048, 2048], P(None, 'tp'), may hold values from -0.125 to 0.125
- write_proj: bfloat16 [2048, 1024], P(None, 'tp'), may hold values from -0.125 to 0.125
- read_proj: bfloat16 [2048, 1024], P(None, 'tp'), may hold values from -0.125 to 0.125
- step_proj: bfloat16 [2048, 2, 32], replicated, may hold values from -0.125 to 0.125
- decay_rate: float32 [2, 32], replicated, may hold values from 3.0456543e-05 to 0.0601
- pacing: float32 [2, 16384], P('dp'), may hold values from 0.2 to 4.3
- value_taps: float32 [5, 2048], replicated, may hold values from -2.5 to 2.5
- write_taps: float32 [5, 1024], replicated, may hold values from -2.5 to 2.5
- read_taps: float32 [5, 1024], replicated, may hold values from -2.5 to 2.5
- norm_gain: float32 [2048], replicated, may hold values from 0.1 to 1.9
- out_proj: bfloat16 [2048, 2048], P('tp'), may hold values from -0.125 to 0.125
Outputs:
- updated: bfloat16 [2, 16384, 2048], P('dp', ('sp', 'tp'))
All inputs are finite; a program needn't handle non-finite values.
Results may differ from a plain program's by a relative error of at most 0.006.
Values may be sent and summed in bfloat16 or wider, within the bound.
A program may use at most 128 MiB of HBM per device.

v0:
```python
import jax
import jax.numpy as jnp
from jax import lax
from jax.sharding import Mesh
from jax.sharding import PartitionSpec as P

HEAD = 64
STATE = 128
ROW = 64
BLOCK = 128
SP = ("sp_0", "sp_1")
SP_TP = ("sp_0", "sp_1", "tp")
NORM_FLOOR = 1e-05
GATED_FLOOR = 1e-06


def over_axes(value, axes):
    for axis in axes:
        value = lax.psum(value, axis)
    return value


def sent_together(arrays, axis, dim, along):
    widths = [a.shape[along] for a in arrays]
    both = jnp.concatenate(arrays, axis=along)
    result = lax.all_gather(both, axis, axis=dim, tiled=True)
    return tuple(jnp.split(result, [sum(widths[:k]) for k in range(1, len(widths))], axis=along))


def cut_along(value, dim, length):
    dims = value.shape
    pieces = value.reshape(*dims[:dim], length, dims[dim] // length, *dims[dim + 1 :])
    return jnp.moveaxis(pieces, dim, 0)


def sum_at_owner(value, axis, dim):
    pieces = cut_along(value, dim, lax.axis_size(axis))
    arrived = lax.all_to_all(pieces, axis, split_axis=0, concat_axis=0, tiled=True)
    return arrived.astype(jnp.float32).sum(axis=0)


def masked_exp(exponent, allowed):
    return jnp.where(allowed, jnp.exp(jnp.where(allowed, exponent, 0.0)), 0.0)


def modulate(row_block, shift_row, scale_row):
    values = row_block.astype(jnp.float32)
    center = jnp.mean(values, -1, keepdims=True)
    spread = jnp.mean(jnp.square(values - center), -1, keepdims=True)
    normed = (values - center) * lax.rsqrt(spread + NORM_FLOOR)
    return (normed * (1.0 + shift_row * 0.0 + scale_row) + shift_row).astype(jnp.bfloat16)


def convolve(values, kernel, run_count):
    length, channels = values.shape
    tap_count = kernel.shape[0]
    margin = tap_count // 2
    stretch = length // run_count
    blocked = values.astype(jnp.float32).reshape(run_count, stretch, channels)
    padded = jnp.pad(blocked, ((0, 0), (margin, margin), (0, 0)))
    summed = jnp.zeros_like(blocked)
    for offset in range(tap_count):
        summed = summed + padded[:, offset : offset + stretch] * kernel[offset]
    return jax.nn.silu(summed).reshape(length, channels).astype(jnp.bfloat16)


def context_state(values, writes, weight, groups):
    length = values.shape[0]
    per_group = weight.shape[1] // groups
    scaled = (
        writes.reshape(length, groups, 1, STATE) * weight.reshape(length, groups, per_group, 1)
    ).astype(jnp.bfloat16)
    head_values = values.reshape(length, groups, per_group, HEAD)
    return jnp.einsum("lgrn,lgrp->grnp", scaled, head_values, preferred_element_type=jnp.float32)


def block_inputs(values, writes, decays, steps, groups):
    length = values.shape[0]
    per_group = decays.shape[1] // groups
    blocks = length // BLOCK
    head_values = values.reshape(blocks, BLOCK, groups, per_group, HEAD)
    write_rows = writes.reshape(blocks, BLOCK, groups, STATE)
    cumulative = jnp.cumsum(decays.reshape(blocks, BLOCK, groups, per_group), axis=1)
    step_rows = steps.reshape(blocks, BLOCK, groups, per_group)
    weight = jnp.exp(cumulative[:, -1:] - cumulative) * step_rows
    scaled = (write_rows[:, :, :, None, :] * weight[..., None]).astype(jnp.bfloat16)
    increment = jnp.einsum(
        "kqgrn,kqgrp->kgrnp", scaled, head_values, preferred_element_type=jnp.float32
    )

    def advance(carry_state, paired):
        block_decay, block_increment = paired
        return (jnp.exp(block_decay)[..., None, None] * carry_state + block_increment, carry_state)

    empty_state = jnp.zeros(increment.shape[1:], jnp.float32)
    final_state, before = lax.scan(advance, empty_state, (cumulative[:, -1], increment))
    return (cumulative, final_state, before)


def block_outputs(values, reads, affinity, cumulative, steps, before, start):
    blocks, block_rows, groups, per_group = cumulative.shape
    head_values = values.reshape(blocks, block_rows, groups, per_group, HEAD)
    read_rows = reads.reshape(blocks, block_rows, groups, STATE).astype(jnp.float32)
    step_rows = steps.reshape(blocks, block_rows, groups, per_group)
    lower_mask = jnp.tril(jnp.ones((block_rows, block_rows), bool))[:, :, None, None]
    exponent = cumulative[:, :, None] - cumulative[:, None, :]
    mixing = (affinity[..., None] * masked_exp(exponent, lower_mask) * step_rows[:, None]).astype(
        jnp.bfloat16
    )
    within = jnp.einsum(
        "ktsgr,ksgrp->ktgrp", mixing, head_values, preferred_element_type=jnp.float32
    )
    block_decay = cumulative[:, -1]
    earlier = jnp.cumsum(block_decay, axis=0) - block_decay
    entering = before + jnp.exp(earlier)[..., None, None] * start[None]
    carried = jnp.einsum("ktgn,kgrnp->ktgrp", read_rows, entering) * jnp.exp(cumulative)[..., None]
    return (within + carried).reshape(blocks * block_rows, groups * per_group * HEAD)


def per_device(
    latent,
    condition,
    context,
    context_cond,
    shift_matrix,
    scale_matrix,
    gate_matrix,
    value_proj,
    gate_proj,
    write_proj,
    read_proj,
    step_proj,
    decay_rate,
    pacing,
    value_taps,
    write_taps,
    read_taps,
    norm_gain,
    out_proj,
):
    sp_count = lax.axis_size(SP)
    sp_index = lax.axis_index(SP)
    tp_index = lax.axis_index("tp")
    model_width = latent.shape[2]
    width_dev = value_proj.shape[1]
    keys_dev = write_proj.shape[1]
    heads_dev = width_dev // HEAD
    groups_dev = keys_dev // STATE
    state_shape = (groups_dev, heads_dev // groups_dev, STATE, HEAD)
    row_share = shift_matrix.shape[0]
    activated = jax.nn.silu(jnp.stack([condition[0], context_cond])).astype(jnp.bfloat16)
    own_cols = lax.dynamic_slice_in_dim(
        activated, (sp_index * lax.axis_size("tp") + tp_index) * row_share, row_share, 1
    )
    shift_part = jnp.dot(own_cols, shift_matrix, preferred_element_type=jnp.float32)
    scale_part = jnp.dot(own_cols, scale_matrix, preferred_element_type=jnp.float32)
    gate_part = jnp.dot(own_cols[:1], gate_matrix, preferred_element_type=jnp.float32)
    shifts, scales, gate_row = (
        over_axes(shift_part, SP_TP),
        over_axes(scale_part, SP_TP),
        over_axes(gate_part, SP_TP),
    )
    step_cols = lax.dynamic_slice_in_dim(step_proj, tp_index * heads_dev, heads_dev, 2).reshape(
        model_width, 2 * heads_dev
    )
    own_rows = modulate(latent[0], shifts[0], scales[0])
    row_piece = lax.all_gather(own_rows, "tp", axis=0, tiled=True)
    projected = jnp.concatenate(
        [
            jnp.dot(row_piece, value_proj, preferred_element_type=jnp.float32),
            jnp.dot(row_piece, gate_proj, preferred_element_type=jnp.float32),
            jnp.dot(row_piece, write_proj, preferred_element_type=jnp.float32),
            jnp.dot(row_piece, read_proj, preferred_element_type=jnp.float32),
            jnp.dot(row_piece, step_cols, preferred_element_type=jnp.float32),
        ],
        axis=1,
    )
    tokens = projected.shape[0]
    run_count = tokens // ROW
    gate_end = 2 * width_dev
    write_end = gate_end + keys_dev
    read_end = write_end + keys_dev
    value_kernel = lax.dynamic_slice_in_dim(value_taps, tp_index * width_dev, width_dev, 1)
    write_kernel = lax.dynamic_slice_in_dim(write_taps, tp_index * keys_dev, keys_dev, 1)
    read_kernel = lax.dynamic_slice_in_dim(read_taps, tp_index * keys_dev, keys_dev, 1)
    values = convolve(projected[:, :width_dev].astype(jnp.bfloat16), value_kernel, run_count)
    gate_pre = projected[:, width_dev:gate_end].astype(jnp.bfloat16)
    writes = convolve(
        projected[:, gate_end:write_end].astype(jnp.bfloat16), write_kernel, run_count
    )
    reads = convolve(projected[:, write_end:read_end].astype(jnp.bfloat16), read_kernel, run_count)
    step_raw = projected[:, read_end:].astype(jnp.bfloat16)
    latent_raw = (
        lax.optimization_barrier(step_raw).astype(jnp.float32).reshape(tokens, 2, heads_dev)
    )
    rates = lax.dynamic_slice_in_dim(decay_rate, tp_index * heads_dev, heads_dev, 1)
    local_pace = lax.dynamic_slice_in_dim(pacing[0], sp_index * tokens, tokens, 0)
    forward_step = jax.nn.softplus(latent_raw[:, 0]) * local_pace[:, None]
    forward_decay = -rates[0][None, :] * forward_step
    backward_step = jax.nn.softplus(latent_raw[:, 1]) * local_pace[:, None]
    backward_decay = -rates[1][None, :] * backward_step
    forward_cumul, forward_end, forward_before = block_inputs(
        values, writes, forward_decay, forward_step, groups_dev
    )
    backward_cumul, backward_end, backward_before = block_inputs(
        values[::-1], writes[::-1], backward_decay[::-1], backward_step[::-1], groups_dev
    )
    context_hidden = modulate(context[0], shifts[1], scales[1])
    context_value = jnp.dot(context_hidden, value_proj, preferred_element_type=jnp.float32).astype(
        jnp.bfloat16
    )
    context_write = jnp.dot(context_hidden, write_proj, preferred_element_type=jnp.float32).astype(
        jnp.bfloat16
    )
    context_raw = jnp.dot(context_hidden, step_cols, preferred_element_type=jnp.float32).astype(
        jnp.bfloat16
    )
    ctx_value_all, ctx_write_all, ctx_raw_all, latent_raw_all = (
        *sent_together((context_value, context_write, context_raw), SP, 0, 1),
        lax.all_gather(step_raw, SP, axis=0, tiled=True),
    )
    ctx_values = convolve(ctx_value_all, value_kernel, 1)
    ctx_writes = convolve(ctx_write_all, write_kernel, 1)
    ctx_raw = lax.optimization_barrier(ctx_raw_all).astype(jnp.float32).reshape(-1, 2, heads_dev)
    ctx_fwd_step = jax.nn.softplus(ctx_raw[:, 0])
    ctx_fwd_decay = -rates[0][None, :] * ctx_fwd_step
    ctx_cumul = jnp.cumsum(ctx_fwd_decay, axis=0)
    ctx_forward = context_state(
        ctx_values, ctx_writes, jnp.exp(ctx_cumul[-1:] - ctx_cumul) * ctx_fwd_step, groups_dev
    )
    ctx_bwd_step = jax.nn.softplus(ctx_raw[:, 1])
    ctx_bwd_decay = -rates[1][None, :] * ctx_bwd_step
    ctx_back_cumul = jnp.cumsum(ctx_bwd_decay, axis=0)
    ctx_backward = context_state(
        ctx_values, ctx_writes, jnp.exp(ctx_back_cumul - ctx_bwd_decay) * ctx_bwd_step, groups_dev
    )
    ctx_forward = ctx_forward.reshape(heads_dev, STATE, HEAD)
    ctx_backward = ctx_backward.reshape(heads_dev, STATE, HEAD)
    empty_state = jnp.zeros((heads_dev, STATE, HEAD), jnp.float32)
    all_raw = (
        lax.optimization_barrier(latent_raw_all)
        .astype(jnp.float32)
        .reshape(sp_count, tokens, 2, heads_dev)
    )
    all_steps = jax.nn.softplus(all_raw) * pacing[0].reshape(sp_count, tokens)[:, :, None, None]
    totals = jnp.sum(-rates[None, None] * all_steps, axis=1)
    forward_totals = totals[:, 0]
    backward_totals = totals[:, 1]
    forward_prefix = jnp.cumsum(forward_totals, axis=0) - forward_totals
    backward_suffix = jnp.cumsum(backward_totals[::-1], axis=0)[::-1] - backward_totals
    forward_through = forward_prefix + forward_totals
    backward_through = backward_suffix + backward_totals
    own_prefix = forward_prefix[sp_index]
    own_suffix = backward_suffix[sp_index]
    forward_piece, backward_piece = tuple(
        (
            part.astype(jnp.float32)
            for part in sent_together(
                (
                    forward_end.reshape(1, heads_dev, STATE, HEAD).astype(jnp.bfloat16),
                    backward_end.reshape(1, heads_dev, STATE, HEAD).astype(jnp.bfloat16),
                ),
                SP,
                0,
                1,
            )
        )
    )
    shard_count = forward_piece.shape[0]
    sources = jnp.arange(shard_count)
    forward_gap = own_prefix[None] - forward_through
    backward_gap = own_suffix[None] - backward_through
    forward_weight = masked_exp(forward_gap, (sources < sp_index)[:, None])
    backward_weight = masked_exp(backward_gap, (sources > sp_index)[:, None])
    forward_in = empty_state + jnp.sum(forward_weight[:, :, None, None] * forward_piece, axis=0)
    backward_in = empty_state + jnp.sum(backward_weight[:, :, None, None] * backward_piece, axis=0)
    forward_start = forward_in + jnp.exp(own_prefix)[:, None, None] * ctx_forward
    backward_start = backward_in + jnp.exp(own_suffix)[:, None, None] * ctx_backward
    blocks = tokens // BLOCK
    forward_affinity = jnp.einsum(
        "ktgn,ksgn->ktsg",
        reads.reshape(blocks, BLOCK, groups_dev, STATE),
        writes.reshape(blocks, BLOCK, groups_dev, STATE),
        preferred_element_type=jnp.float32,
    )
    backward_affinity = forward_affinity[::-1, ::-1, ::-1]
    forward_out = block_outputs(
        values,
        reads,
        forward_affinity,
        forward_cumul,
        forward_step,
        forward_before,
        forward_start.reshape(state_shape),
    )
    backward_out = block_outputs(
        values[::-1],
        reads[::-1],
        backward_affinity,
        backward_cumul,
        backward_step[::-1],
        backward_before,
        backward_start.reshape(state_shape),
    )[::-1]
    gated_heads = (forward_out + backward_out) * jax.nn.silu(gate_pre.astype(jnp.float32))
    grouped = gated_heads.reshape(tokens, groups_dev, -1)
    grouped = grouped * lax.rsqrt(jnp.mean(grouped * grouped, -1, keepdims=True) + GATED_FLOOR)
    gain_dev = lax.dynamic_slice_in_dim(norm_gain, tp_index * width_dev, width_dev, 0)
    inner_rows = (grouped.reshape(tokens, width_dev) * gain_dev).astype(jnp.bfloat16)
    mixed = sum_at_owner(
        jnp.dot(inner_rows, out_proj, preferred_element_type=jnp.float32).astype(jnp.bfloat16),
        "tp",
        0,
    ).astype(jnp.bfloat16)
    updated = (
        latent[0].astype(jnp.float32)
        + gate_row[0] * lax.optimization_barrier(mixed).astype(jnp.float32)
    ).astype(jnp.bfloat16)
    return updated[None]


def solution(mesh):
    torus = Mesh(
        mesh.devices.reshape(8, 4, mesh.shape["tp"], mesh.shape["dp"]), ("sp_0", "sp_1", "tp", "dp")
    )
    placed = (
        P("dp", SP_TP, None),
        P("dp", None),
        P("dp", SP, None),
        P(),
        P(SP_TP, None),
        P(SP_TP, None),
        P(SP_TP, None),
        P(None, "tp"),
        P(None, "tp"),
        P(None, "tp"),
        P(None, "tp"),
        P(),
        P(),
        P("dp", None),
        P(),
        P(),
        P(),
        P(),
        P("tp", None),
    )
    return jax.shard_map(
        per_device, mesh=torus, in_specs=placed, out_specs=P("dp", SP_TP, None), check_vma=False
    )
```

profile of v0, /device:TPU:8, one launch (start us, length us, event | category | flops | bytes accessed | tf_op | source)
XLA Modules:
  0.0 367.3 jit_solution(16203024841715670939)
XLA Ops:
  13.0 33.2 %all-reduce.5 = (f32[2,2048]{1,0:T(2,128)S(1)}, f32[2,2048]{1,0:T(2,128)S(1)}, f32[1,2048]{1,0:T(1,128)S(1)}) all-reduce(f32[2,2048]{1,0:T(2,128)S(1)} %fusion.172, f32[2,2048]{1,0:T(2,128)S(1)} %fusion.173, f32[1,2048]{1,0:T(1,128)S(1)} %fusion.153), channel_id=1, replica_groups=mesh['sp_0'=8,'sp_1'=4,'tp'=4,'dp'=2] {'sp_0'}, use_global_device_ids=true, to_apply=%region_5.6 | all-reduce | flops 10240 | bytes 81920 | tf_op jit(solution)/shard_map/psum | solution.py:19
  46.1 17.4 %all-reduce.7 = (f32[2,2048]{1,0:T(2,128)S(1)}, f32[2,2048]{1,0:T(2,128)S(1)}, f32[1,2048]{1,0:T(1,128)S(1)}) all-reduce(f32[2,2048]{1,0:T(2,128)S(1)} %get-tuple-element.183, f32[2,2048]{1,0:T(2,128)S(1)} %get-tuple-element.184, f32[1,2048]{1,0:T(1,128)S(1)} %get-tuple-element.185), channel_id=1, replica_groups=mesh['sp_0'=8,'sp_1'=4,'tp'=4,'dp'=2] {'sp_1'}, use_global_device_ids=true, to_apply=%region_6.7 | all-reduce | flops 10240 | bytes 81920 | tf_op jit(solution)/shard_map/psum | solution.py:19
  63.5 15.2 %all-reduce.6 = (f32[2,2048]{1,0:T(2,128)S(1)}, f32[2,2048]{1,0:T(2,128)S(1)}, f32[2048]{0:T(1024)}) all-reduce(f32[2,2048]{1,0:T(2,128)S(1)} %get-tuple-element.189, f32[2,2048]{1,0:T(2,128)S(1)} %get-tuple-element.190, f32[2048]{0:T(1024)S(1)} %bitcast.366), channel_id=1, replica_groups=mesh['sp_0'=8,'sp_1'=4,'tp'=4,'dp'=2] {'tp'}, use_global_device_ids=true, to_apply=%region_7.8 | all-reduce | flops 10240 | bytes 81920 | tf_op jit(solution)/shard_map/psum | solution.py:19
  78.7 2.2 fusion.60
  82.9 2.1 convolution_convert_fusion.5
  89.2 1.7 constant_dynamic-slice_fusion.5
  91.0 20.2 %all-gather.4.cloned.1.call-done = bf16[512,2048]{1,0:T(8,128)(2,1)} async-done(((bf16[128,2048]{1,0:T(8,128)(2,1)}), bf16[512,2048]{1,0:T(8,128)(2,1)}) %all-gather.4.cloned.1.call-update) | async-done | bytes 2097168 | tf_op jit(solution)/shard_map/all_gather | solution.py:167
  111.2 2.2 convolution_convert_fusion.7
  118.4 2.7 fusion.169
  122.3 3.5 convolution_convert_fusion.2
  127.6 8.3 %rev.32 = bf16[512,512]{1,0:T(8,128)(2,1)} reverse(bf16[512,512]{1,0:T(8,128)(2,1)} %bitcast.310), dimensions={0} | reverse | bytes 1048576 | tf_op jit(solution)/shard_map/rev | solution.py:206
  135.9 2.9 reshape.563
  138.9 2.3 copy.245
  141.2 2.6 convolution_convert_fusion.4
  144.2 2.6 rev.30
  146.9 2.0 reshape.554
  150.0 3.6 fusion.75
  155.2 8.1 %while.27 = (s32[]{:T(128)}, f32[2,4,128,64]{3,2,1,0:T(8,128)S(1)}, f32[4,2,4,128,64]{4,3,2,1,0:T(8,128)}, f32[4,2,4]{2,1,0:T(2,128)S(1)}, f32[4,2,4,128,64]{4,3,2,1,0:T(8,128)}, /*index=5*/s32[]{:T(128)}, s32[]{:T(128)}) while((s32[]{:T(128)}, f32[2,4,128,64]{3,2,1,0:T(8,128)S(1)}, f32[4,2,4,128,64]{4,3,2,1,0:T(8,128)}, ...), condition=%wide.region_19.20_spmd.clone, body=%wide.region_18.19_spmd.clone.sunk | while | flops 262147 | bytes 1573568 | solution.py:96
  167.7 1.8 copy.232
  169.6 2.9 reshape.562
  175.3 1.7 copy.234
  178.0 2.6 fusion.74
  180.6 1.6 broadcast.242.clone.1
  182.2 10.8 %while.26 = (s32[]{:T(128)}, f32[2,4,128,64]{3,2,1,0:T(8,128)S(1)}, f32[4,2,4,128,64]{4,3,2,1,0:T(8,128)}, f32[4,2,4]{2,1,0:T(2,128)}, f32[4,2,4,128,64]{4,3,2,1,0:T(8,128)}, /*index=5*/s32[]{:T(128)}, s32[]{:T(128)}) while((s32[]{:T(128)}, f32[2,4,128,64]{3,2,1,0:T(8,128)S(1)}, f32[4,2,4,128,64]{4,3,2,1,0:T(8,128)}, ...), condition=%wide.region_13.14_spmd.clone, body=%wide.region_12.13_spmd.clone.sunk | while | flops 262147 | bytes 1573568 | solution.py:96
  200.2 2.3 reduce-window.16
  202.8 2.3 reduce-window.14
  206.4 2.3 split.21
  208.7 1.7 copy.289
  211.6 2.8 fusion.118
  214.4 2.7 reshape.555
  217.2 2.3 copy.251
  220.4 3.8 %multiply_convert_fusion.5 = bf16[1,1024,512]{1,2,0:T(8,128)(2,1)} fusion(f32[1,1024,512]{1,2,0:T(8,128)S(1)} %convert_bitcast_fusion, bf16[1024,512]{0,1:T(8,128)(2,1)S(1)} %copy.289, f32[512]{0:T(512)S(1)} %bitcast.351, f32[512]{0:T(512)S(1)} %bitcast.345, f32[512]{0:T(512)S(1)} %bitcast.347, f32[512]{0:T(512)S(1)} %bitcast.349, f32[512]{0:T(512)S(1)} %bitcast.343), kind=kLoop, calls=%fused_computation.37 | loop fusion | flops 7864320 | bytes 4204544 | tf_op jit(solution)/shard_map/convert_element_type | solution.py:64
  230.3 3.0 rev.33
  234.1 51.8 %all_gather.13 = bf16[16384,16]{0,1:T(8,128)(2,1)S(1)} all-gather(bf16[512,16]{0,1:T(8,128)(2,1)S(1)} %convolution_convert_fusion.7), channel_id=1, replica_groups=mesh['sp_0'=8,'sp_1'=4,'tp'=4,'dp'=2] {'sp_0','sp_1'}, dimensions={0}, use_global_device_ids=true | all-gather | bytes 540672 | tf_op jit(solution)/shard_map/all_gather | solution.py:220
  292.5 2.0 copy.260
  295.7 2.9 rev.36
  298.6 1.7 reshape.541
  303.1 2.9 convolution_bitcast_fusion.1
  306.1 1.9 convolution_bitcast_fusion
  308.0 4.5 %multiply_reduce_fusion.1 = (f32[8,128,64]{1,2,0:T(8,128)S(1)}, f32[8,128,64]{1,2,0:T(8,128)S(1)}) fusion(bf16[32,16,128,64]{2,3,1,0:T(8,128)(2,1)} %all-gather.6.cloned.1.call-done, f32[32,8]{1,0:T(8,128)S(1)} %exponential_select_fusion.1, f32[32,8]{1,0:T(8,128)S(1)} %get-tuple-element.211), kind=kLoop, calls=%fused_computation.7 | loop fusion | flops 12451840 | bytes 8914944 | tf_op jit(solution)/shard_map/reduce_sum | solution.py:275
  314.5 2.6 fusion.27
  317.1 1.7 copy.259
  318.8 1.6 fusion.44
  320.6 2.6 fusion.36
  324.0 6.0 %rev.37 = f32[512,512]{0,1:T(8,128)} reverse(f32[512,512]{0,1:T(8,128)S(1)} %bitcast.312), dimensions={0} | reverse | bytes 2097152 | tf_op jit(solution)/shard_map/rev | solution.py:296
  329.9 4.3 %bitcast_reduce_fusion = (f32[512,2]{0,1:T(2,128)S(1)}, f32[512,512]{0,1:T(8,128)S(1)}) fusion(bf16[512,2048]{1,0:T(8,128)(2,1)} %all-gather.4.cloned.1.call-done, bf16[2048,512]{1,0:T(8,128)(2,1)} %param.31, f32[512,512]{0,1:T(8,128)} %rev.37, f32[64,8,4,128]{3,2,1,0:T(4,128)} %bitcast.318), kind=kOutput, calls=%fused_computation.119 | convolution fusion | flops 1076362240 | bytes 7344128 | tf_op jit(solution)/shard_map/dot_general | solution.py:171
  335.8 21.9 %all_to_all.5 = bf16[4,128,2048]{2,1,0:T(8,128)(2,1)} all-to-all(bf16[4,128,2048]{2,1,0:T(8,128)(2,1)S(1)} %bitcast.316), channel_id=1, replica_groups=mesh['sp_0'=8,'sp_1'=4,'tp'=4,'dp'=2] {'tp'}, dimensions={0} | all-to-all | bytes 4194304 | tf_op jit(solution)/shard_map/all_to_all | solution.py:38
  357.7 2.1 reduce_sum.98
  (284 shorter events, 83.6 us)
Async XLA Ops:
  6.5 328.0 %copy-start = (bf16[512,2048]{1,0:T(8,128)(2,1)S(1)}, bf16[512,2048]{1,0:T(8,128)(2,1)}, u32[]{:S(2)}) copy-start(bf16[512,2048]{1,0:T(8,128)(2,1)} %param.41) | copy-start | bytes 6291460
  6.5 74.5 %copy-start.14 = (bf16[1,32,2048]{2,1,0:T(8,128)(2,1)S(1)}, bf16[1,32,2048]{2,1,0:T(8,128)(2,1)}, u32[]{:S(2)}) copy-start(bf16[1,32,2048]{2,1,0:T(8,128)(2,1)} %param.25) | copy-start | bytes 393220
  6.5 76.0 %copy-start.16 = (bf16[2048,256]{1,0:T(8,128)(2,1)S(1)}, bf16[2048,256]{1,0:T(8,128)(2,1)}, u32[]{:S(2)}) copy-start(bf16[2048,256]{1,0:T(8,128)(2,1)} %param.32) | copy-start | bytes 3145732
  6.5 104.7 %all-gather.4.cloned.1.call-start = ((), (), s32[]{:S(2)}) async-start(), calls=%async_computation.1 | async-start | bytes 2621440 | tf_op jit(solution)/shard_map/all_gather | solution.py:167
  81.0 118.0 %all-gather.8.cloned.1.call-start = ((), (), s32[]{:S(2)}) async-start(), calls=%async_computation.3 | async-start | bytes 1892352 | tf_op jit(solution)/shard_map/all_gather | solution.py:26
  81.4 4.4 %copy-start.65 = (f32[2,32]{1,0:T(2,128)S(1)}, f32[2,32]{1,0:T(2,128)}, u32[]{:S(2)}) copy-start(f32[2,32]{1,0:T(2,128)} %param.35) | copy-start | bytes 772
  85.7 222.3 %all-gather.6.cloned.1.call-start = ((), (), s32[]{:S(2)}) async-start(), calls=%async_computation.2 | async-start | bytes 8650752 | tf_op jit(solution)/shard_map/all_gather | solution.py:26
  86.9 31.5 %copy-start.56 = (f32[8]{0:T(128)}, f32[8]{0:T(128)S(1)}, u32[]{:S(2)}) copy-start(f32[8]{0:T(128)S(1)} %get-tuple-element.232) | copy-start | bytes 100
  89.2 36.8 %copy-start.31 = (f32[1,512]{1,0:T(1,128)}, f32[1,512]{1,0:T(1,128)S(1)}, u32[]{:S(2)}) copy-start(f32[1,512]{1,0:T(1,128)S(1)} %get-tuple-element.204) | copy-start | bytes 6148
  89.2 36.8 %copy-start.33 = (f32[1,512]{1,0:T(1,128)}, f32[1,512]{1,0:T(1,128)S(1)}, u32[]{:S(2)}) copy-start(f32[1,512]{1,0:T(1,128)S(1)} %get-tuple-element.205) | copy-start | bytes 6148
  89.2 36.8 %copy-start.35 = (f32[1,512]{1,0:T(1,128)}, f32[1,512]{1,0:T(1,128)S(1)}, u32[]{:S(2)}) copy-start(f32[1,512]{1,0:T(1,128)S(1)} %get-tuple-element.206) | copy-start | bytes 6148
  89.2 36.8 %copy-start.37 = (f32[1,512]{1,0:T(1,128)}, f32[1,512]{1,0:T(1,128)S(1)}, u32[]{:S(2)}) copy-start(f32[1,512]{1,0:T(1,128)S(1)} %get-tuple-element.207) | copy-start | bytes 6148
  89.2 36.8 %copy-start.39 = (f32[1,512]{1,0:T(1,128)}, f32[1,512]{1,0:T(1,128)S(1)}, u32[]{:S(2)}) copy-start(f32[1,512]{1,0:T(1,128)S(1)} %get-tuple-element.208) | copy-start | bytes 6148
  90.9 52.8 %copy-start.45 = (f32[1,256]{1,0:T(1,128)}, f32[1,256]{1,0:T(1,128)S(1)}, u32[]{:S(2)}) copy-start(f32[1,256]{1,0:T(1,128)S(1)} %get-tuple-element.215) | copy-start | bytes 3076
  90.9 52.8 %copy-start.47 = (f32[1,256]{1,0:T(1,128)}, f32[1,256]{1,0:T(1,128)S(1)}, u32[]{:S(2)}) copy-start(f32[1,256]{1,0:T(1,128)S(1)} %get-tuple-element.216) | copy-start | bytes 3076
  91.0 52.8 %copy-start.49 = (f32[1,256]{1,0:T(1,128)}, f32[1,256]{1,0:T(1,128)S(1)}, u32[]{:S(2)}) copy-start(f32[1,256]{1,0:T(1,128)S(1)} %get-tuple-element.217) | copy-start | bytes 3076
  91.0 52.8 %copy-start.51 = (f32[1,256]{1,0:T(1,128)}, f32[1,256]{1,0:T(1,128)S(1)}, u32[]{:S(2)}) copy-start(f32[1,256]{1,0:T(1,128)S(1)} %get-tuple-element.218) | copy-start | bytes 3076
  91.0 52.8 %copy-start.53 = (f32[1,256]{1,0:T(1,128)}, f32[1,256]{1,0:T(1,128)S(1)}, u32[]{:S(2)}) copy-start(f32[1,256]{1,0:T(1,128)S(1)} %get-tuple-element.219) | copy-start | bytes 3076
  113.5 7.6 %copy-start.22 = (f32[512,2,8]{0,2,1:T(8,128)}, f32[512,2,8]{0,2,1:T(8,128)S(1)}, u32[]{:S(2)}) copy-start(f32[512,2,8]{0,2,1:T(8,128)S(1)} %bitcast_convert_fusion.1) | copy-start | bytes 98308
  117.4 8.5 %copy-start.24 = (f32[512,8]{0,1:T(8,128)}, f32[512,8]{0,1:T(8,128)S(1)}, u32[]{:S(2)}) copy-start(f32[512,8]{0,1:T(8,128)S(1)} %rev.31) | copy-start | bytes 49156
  144.2 9.4 %copy-start.7 = (bf16[8,64,256]{2,1,0:T(8,128)(2,1)}, bf16[8,64,256]{2,1,0:T(8,128)(2,1)S(1)}, u32[]{:S(2)}) copy-start(bf16[8,64,256]{2,1,0:T(8,128)(2,1)S(1)} %multiply_convert_fusion.24) | copy-start | bytes 786436
  155.2 8.1 %slice-start = ((f32[512,2,8]{0,2,1:T(8,128)}), f32[512,1,8]{0,2,1:T(8,128)S(1)}, s32[]{:S(2)}) async-start(f32[512,2,8]{0,2,1:T(8,128)} %copy-done.22), calls=%async_computation.4 | async-start | bytes 32768 | tf_op jit(solution)/shard_map/slice | solution.py:198
  155.2 8.1 %copy-start.66 = (f32[2,4]{1,0:T(2,128)S(1)}, f32[2,4]{1,0:T(2,128)}, u32[]{:S(2)}) copy-start(f32[2,4]{1,0:T(2,128)} %mul.730) | copy-start | bytes 100
  177.0 5.2 %copy-start.12 = (bf16[4,128,2,4,64]{1,4,3,2,0:T(8,128)(2,1)}, bf16[4,128,2,4,64]{1,4,3,2,0:T(8,128)(2,1)S(1)}, u32[]{:S(2)}) copy-start(bf16[4,128,2,4,64]{1,4,3,2,0:T(8,128)(2,1)S(1)} %copy.234) | copy-start | bytes 1572868
  182.2 12.3 %copy-start.23 = (f32[1,16384]{1,0:T(1,128)S(1)}, f32[1,16384]{1,0:T(1,128)}, u32[]{:S(2)}) copy-start(f32[1,16384]{1,0:T(1,128)} %param.36) | copy-start | bytes 196612
  193.0 7.0 %copy-start.57 = (f32[8]{0:T(128)S(1)}, f32[8]{0:T(128)}, u32[]{:S(2)}) copy-start(f32[8]{0:T(128)} %copy-done.56) | copy-start | bytes 100
  193.0 7.0 %copy-start.64 = (f32[8]{0:T(128)S(1)}, f32[8]{0:T(128)}, u32[]{:S(2)}) copy-start(f32[8]{0:T(128)} %get-tuple-element.231) | copy-start | bytes 100
  208.7 2.9 copy-start.54
  220.4 3.8 %copy-start.3 = (f32[4,128,2,4]{3,2,1,0:T(2,128)S(1)}, f32[4,128,2,4]{3,2,1,0:T(2,128)}, u32[]{:S(2)}) copy-start(f32[4,128,2,4]{3,2,1,0:T(2,128)} %copy-done.2) | copy-start | bytes 49156
  220.4 4.9 %copy-start.10 = (bf16[512,2048]{1,0:T(8,128)(2,1)S(1)}, bf16[512,2048]{1,0:T(8,128)(2,1)}, u32[]{:S(2)}) copy-start(bf16[512,2048]{1,0:T(8,128)(2,1)} %all-gather.4.cloned.1.call-done) | copy-start | bytes 6291460
  220.4 4.9 %copy-start.67 = (bf16[2048,256]{1,0:T(8,128)(2,1)S(1)}, bf16[2048,256]{1,0:T(8,128)(2,1)}, u32[]{:S(2)}) copy-start(bf16[2048,256]{1,0:T(8,128)(2,1)} %param.33) | copy-start | bytes 3145732
  226.1 7.1 %copy-start.5 = (f32[4,128,2,4]{3,2,1,0:T(2,128)S(1)}, f32[4,128,2,4]{3,2,1,0:T(2,128)}, u32[]{:S(2)}) copy-start(f32[4,128,2,4]{3,2,1,0:T(2,128)} %copy-done.4) | copy-start | bytes 49156
  228.0 57.8 %copy-start.28 = (f32[32,512]{1,0:T(8,128)S(1)}, f32[32,512]{1,0:T(8,128)}, u32[]{:S(2)}) copy-start(f32[32,512]{1,0:T(8,128)} %mul.746) | copy-start | bytes 196612
  234.1 61.7 %copy-start.9 = (bf16[8,64,256]{2,1,0:T(8,128)(2,1)S(1)}, bf16[8,64,256]{2,1,0:T(8,128)(2,1)}, u32[]{:S(2)}) copy-start(bf16[8,64,256]{2,1,0:T(8,128)(2,1)} %copy-done.8) | copy-start | bytes 786436
  285.8 17.2 %copy-start.13 = (bf16[4,128,2,4,64]{1,4,3,2,0:T(8,128)(2,1)S(1)}, bf16[4,128,2,4,64]{1,4,3,2,0:T(8,128)(2,1)}, u32[]{:S(2)}) copy-start(bf16[4,128,2,4,64]{1,4,3,2,0:T(8,128)(2,1)} %copy-done.12) | copy-start | bytes 1572868
  285.9 17.2 %copy-start.26 = (f32[4,128,2,4]{1,3,2,0:T(4,128)S(1)}, f32[4,128,2,4]{1,3,2,0:T(4,128)}, u32[]{:S(2)}) copy-start(f32[4,128,2,4]{1,3,2,0:T(4,128)} %get-tuple-element.195) | copy-start | bytes 49156
  285.9 17.2 %copy-start.27 = (f32[4,128,2,4]{1,3,2,0:T(4,128)S(1)}, f32[4,128,2,4]{1,3,2,0:T(4,128)}, u32[]{:S(2)}) copy-start(f32[4,128,2,4]{1,3,2,0:T(4,128)} %copy.232) | copy-start | bytes 49156
  285.9 17.2 %copy-start.42 = (pred[128,128]{1,0:T(8,128)(4,1)S(1)}, pred[128,128]{1,0:T(8,128)(4,1)}, u32[]{:S(2)}) copy-start(pred[128,128]{1,0:T(8,128)(4,1)} %iota_compare_fusion) | copy-start | bytes 49156
  303.1 3.0 copy-start.11
  303.1 3.0 copy-start.21
  303.1 3.0 copy-start.25
  303.1 3.0 copy-start.41
  308.0 4.6 %copy-start.17 = (f32[1024,2,128]{2,0,1:T(8,128)S(1)}, f32[1024,2,128]{2,0,1:T(8,128)}, u32[]{:S(2)}) copy-start(f32[1024,2,128]{2,0,1:T(8,128)} %copy.251) | copy-start | bytes 3145732
  308.0 4.6 %copy-start.19 = (bf16[1,1024,512]{1,2,0:T(8,128)(2,1)S(1)}, bf16[1,1024,512]{1,2,0:T(8,128)(2,1)}, u32[]{:S(2)}) copy-start(bf16[1,1024,512]{1,2,0:T(8,128)(2,1)} %multiply_convert_fusion.5) | copy-start | bytes 3145732
  308.0 4.6 %copy-start.29 = (f32[1024,2,4]{0,2,1:T(4,128)S(1)}, f32[1024,2,4]{0,2,1:T(4,128)}, u32[]{:S(2)}) copy-start(f32[1024,2,4]{0,2,1:T(4,128)} %mul.790) | copy-start | bytes 98308
  308.0 4.6 %copy-start.69 = (f32[2,4]{1,0:T(2,128)S(1)}, f32[2,4]{1,0:T(2,128)}, u32[]{:S(2)}) copy-start(f32[2,4]{1,0:T(2,128)} %exp.172) | copy-start | bytes 100
  314.5 4.3 %copy-start.30 = (f32[1024,2,4]{0,2,1:T(4,128)S(1)}, f32[1024,2,4]{0,2,1:T(4,128)}, u32[]{:S(2)}) copy-start(f32[1024,2,4]{0,2,1:T(4,128)} %mul.821) | copy-start | bytes 98308
  329.9 4.4 %copy-start.58 = (f32[512]{0:T(512)S(1)}, f32[512]{0:T(512)}, u32[]{:S(2)}) copy-start(f32[512]{0:T(512)} %dynamic_slice.53) | copy-start | bytes 6148
  (26 other events, 39.0 us)
Sparse Core Ops, SparseCore 0:
  81.1 30.1 all-gather.3
  113.8 78.5 all-gather.7
  195.0 100.4 all-gather.5
where the time goes:
time: 371 us; the launch traced here: 367 us
  blocking collectives  139 us (37%)
  local copies, waits for them, and re-layouts  88 us (24%)
  other arithmetic  63.3 us (17%)
  matrix products  41.8 us (11%)
  waiting for transfers between devices  20.3 us (5%)
  between operations  14.3 us (4%)
    psum x3, blocking collectives, over_axes(): value = lax.psum(value, axis)  65.7 us
    all_gather x1, blocking collectives, per_device(): lax.all_gather(step_raw, SP, axis=0, tiled=True)  51.8 us
    all_to_all x1, blocking collectives, sum_at_owner(): lax.all_to_all(pieces, axis, split_axis=0, concat_axis=0, tiled=True)  21.9 us
    all_gather x1, waiting for transfers between devices, per_device(): row_piece = lax.all_gather(own_rows, 'tp', axis=0, tiled=True)  20.2 us
    add x8, other arithmetic, advance(): jnp.exp(block_decay)[..., None, None] * carry_state + block_increment  9.3 us
    rev x1, local copies, waits for them, and re-layouts, per_device(): values[::-1]  8.32 us
  transfers between devices with their start and end apart: 3, of which 1 were waited for; matrix products, arithmetic and copies ran while one was open for 41% of the time, Pallas kernels for 0%

commit v1 on v0

--- a/solution.py
+++ b/solution.py
@@ -16,7 +16,7 @@
 
 def over_axes(value, axes):
     for axis in axes:
-        value = lax.psum(value, axis)
+        value = lax.all_gather(value, axis_name=axis).sum(axis=0)
     return value
 
 

time: 371 us -> 439 us (1.18)
  blocking collectives: 139 us -> 202 us
  starting transfers between devices: 0.09 us -> 6.09 us
    all_gather x0 -> x9, blocking collectives: none -> 150 us  [over_axes(): value = lax.all_gather(value, axis_name=axis).sum(axis=0)]
    psum x3 -> x0, blocking collectives: 65.7 us -> none  [over_axes(): value = lax.psum(value, axis)]
    all_to_all x1 -> x0, blocking collectives: 21.9 us -> none  [sum_at_owner(): lax.all_to_all(pieces, axis, split_axis=0, concat_axis=0, tiled=True)]
    all_to_all x0 -> x1, starting transfers between devices: none -> 6 us  [sum_at_owner(): lax.all_to_all(pieces, axis, split_axis=0, concat_axis=0, tiled=True)]
  transfers between devices with their start and end apart: 3 -> 4, of which waited for: 1 -> 1; matrix products, arithmetic and copies ran while one was open for 41% -> 35% of each run, Pallas kernels for 0% -> 0%
where the time goes in v1:
time: 439 us; the launch traced here: 435 us
  blocking collectives  202 us (46%)
  local copies, waits for them, and re-layouts  84.3 us (19%)
  other arithmetic  64.1 us (15%)
  matrix products  44 us (10%)
  waiting for transfers between devices  20.8 us (5%)
  between operations  14.2 us (3%)
  starting transfers between devices  6.09 us (1%)
    all_gather x9, blocking collectives, over_axes(): value = lax.all_gather(value, axis_name=axis).sum(axis=0)  150 us
    all_gather x1, blocking collectives, per_device(): lax.all_gather(step_raw, SP, axis=0, tiled=True)  52.2 us
    all_gather x1, waiting for transfers between devices, per_device(): row_piece = lax.all_gather(own_rows, 'tp', axis=0, tiled=True)  20.7 us
    add x8, other arithmetic, advance(): jnp.exp(block_decay)[..., None, None] * carry_state + block_increment  9.3 us
  transfers between devices with their start and end apart: 4, of which 1 were waited for; matrix products, arithmetic and copies ran while one was open for 35% of the time, Pallas kernels for 0%

profile of v1, /device:TPU:8, one launch (start us, length us, event | category | flops | bytes accessed | tf_op | source)
XLA Modules:
  0.0 435.4 jit_solution(7170426092652810444)
XLA Ops:
  8.4 28.3 %all-gather.12 = f32[8,2,2048]{2,1,0:T(2,128)S(1)} all-gather(f32[1,2,2048]{2,1,0:T(2,128)S(1)} %convolution_bitcast_fusion), channel_id=8, replica_groups=mesh['sp_0'=8,'sp_1'=4,'tp'=4,'dp'=2] {'sp_0'}, dimensions={0}, use_global_device_ids=true | all-gather | bytes 147456 | tf_op jit(solution)/shard_map/all_gather | solution.py:19
  36.8 12.3 %all-gather.13 = f32[4,2,2048]{2,1,0:T(2,128)S(1)} all-gather(f32[1,2,2048]{2,1,0:T(2,128)S(1)} %bitcast.343), channel_id=9, replica_groups=mesh['sp_0'=8,'sp_1'=4,'tp'=4,'dp'=2] {'sp_1'}, dimensions={0}, use_global_device_ids=true | all-gather | bytes 81920 | tf_op jit(solution)/shard_map/all_gather | solution.py:19
  49.1 12.1 %all-gather.14 = f32[4,2,2048]{2,1,0:T(2,128)S(1)} all-gather(f32[1,2,2048]{2,1,0:T(2,128)S(1)} %bitcast.344), channel_id=10, replica_groups=mesh['sp_0'=8,'sp_1'=4,'tp'=4,'dp'=2] {'tp'}, dimensions={0}, use_global_device_ids=true | all-gather | bytes 81920 | tf_op jit(solution)/shard_map/all_gather | solution.py:19
  62.2 24.6 %all-gather.9 = f32[8,2,2048]{2,1,0:T(2,128)S(1)} all-gather(f32[1,2,2048]{2,1,0:T(2,128)S(1)} %convolution_bitcast_fusion.1), channel_id=5, replica_groups=mesh['sp_0'=8,'sp_1'=4,'tp'=4,'dp'=2] {'sp_0'}, dimensions={0}, use_global_device_ids=true | all-gather | bytes 147456 | tf_op jit(solution)/shard_map/all_gather | solution.py:19
  86.8 11.9 %all-gather.10 = f32[4,2,2048]{2,1,0:T(2,128)S(1)} all-gather(f32[1,2,2048]{2,1,0:T(2,128)S(1)} %bitcast.345), channel_id=6, replica_groups=mesh['sp_0'=8,'sp_1'=4,'tp'=4,'dp'=2] {'sp_1'}, dimensions={0}, use_global_device_ids=true | all-gather | bytes 81920 | tf_op jit(solution)/shard_map/all_gather | solution.py:19
  98.7 11.9 %all-gather.11 = f32[4,2,2048]{2,1,0:T(2,128)S(1)} all-gather(f32[1,2,2048]{2,1,0:T(2,128)S(1)} %bitcast.346), channel_id=7, replica_groups=mesh['sp_0'=8,'sp_1'=4,'tp'=4,'dp'=2] {'tp'}, dimensions={0}, use_global_device_ids=true | all-gather | bytes 81920 | tf_op jit(solution)/shard_map/all_gather | solution.py:19
  115.8 2.1 convolution_convert_fusion.5
  123.4 20.7 %all-gather.19.cloned.1.call-done = bf16[512,2048]{1,0:T(8,128)(2,1)} async-done(((bf16[128,2048]{1,0:T(8,128)(2,1)}), bf16[512,2048]{1,0:T(8,128)(2,1)}) %all-gather.19.cloned.1.call-update) | async-done | bytes 2097168 | tf_op jit(solution)/shard_map/all_gather | solution.py:167
  144.1 3.5 convolution_convert_fusion.2
  149.3 8.3 %rev.32 = bf16[512,512]{1,0:T(8,128)(2,1)} reverse(bf16[512,512]{1,0:T(8,128)(2,1)} %bitcast.317), dimensions={0} | reverse | bytes 1048576 | tf_op jit(solution)/shard_map/rev | solution.py:206
  157.6 2.9 reshape.600
  160.6 2.3 copy.295
  162.9 2.2 convolution_convert_fusion.7
  168.1 2.8 convolution_convert_fusion.4
  172.8 2.7 fusion.169
  176.7 2.5 multiply_convert_fusion.24
  179.3 2.6 rev.30
  181.9 2.0 reshape.561
  185.0 3.7 fusion.75
  190.2 8.1 %while.27 = (s32[]{:T(128)}, f32[2,4,128,64]{3,2,1,0:T(8,128)S(1)}, f32[4,2,4,128,64]{4,3,2,1,0:T(8,128)}, f32[4,2,4]{2,1,0:T(2,128)S(1)}, f32[4,2,4,128,64]{4,3,2,1,0:T(8,128)}, /*index=5*/s32[]{:T(128)}, s32[]{:T(128)}) while((s32[]{:T(128)}, f32[2,4,128,64]{3,2,1,0:T(8,128)S(1)}, f32[4,2,4,128,64]{4,3,2,1,0:T(8,128)}, ...), condition=%wide.region_19.20_spmd.clone, body=%wide.region_18.19_spmd.clone.sunk | while | flops 262147 | bytes 1573068 | solution.py:96
  203.7 3.0 reshape.599
  213.1 2.6 fusion.74
  217.3 10.8 %while.26 = (s32[]{:T(128)}, f32[2,4,128,64]{3,2,1,0:T(8,128)S(1)}, f32[4,2,4,128,64]{4,3,2,1,0:T(8,128)}, f32[4,2,4]{2,1,0:T(2,128)}, f32[4,2,4,128,64]{4,3,2,1,0:T(8,128)}, /*index=5*/s32[]{:T(128)}, s32[]{:T(128)}) while((s32[]{:T(128)}, f32[2,4,128,64]{3,2,1,0:T(8,128)S(1)}, f32[4,2,4,128,64]{4,3,2,1,0:T(8,128)}, ...), condition=%wide.region_13.14_spmd.clone, body=%wide.region_12.13_spmd.clone.sunk | while | flops 262147 | bytes 1573068 | solution.py:96
  233.5 2.3 split.21
  237.5 2.3 reduce-window.16
  240.1 2.5 reduce-window.14
  245.6 2.8 fusion.118
  248.5 2.8 reshape.562
  251.2 2.3 copy.301
  254.4 3.8 multiply_convert_fusion.5
  260.1 2.6 convolution_convert_fusion.3
  266.0 3.0 rev.33
  271.1 2.0 copy.310
  273.1 52.2 %all_gather.85 = bf16[16384,16]{0,1:T(8,128)(2,1)S(1)} all-gather(bf16[512,16]{0,1:T(8,128)(2,1)S(1)} %convolution_convert_fusion.7), channel_id=1, replica_groups=mesh['sp_0'=8,'sp_1'=4,'tp'=4,'dp'=2] {'sp_0','sp_1'}, dimensions={0}, use_global_device_ids=true | all-gather | bytes 540672 | tf_op jit(solution)/shard_map/all_gather | solution.py:220
  329.3 2.9 rev.36
  337.0 3.0 convolution_bitcast_fusion.3
  341.9 4.5 %multiply_reduce_fusion.1 = (f32[8,128,64]{1,2,0:T(8,128)S(1)}, f32[8,128,64]{1,2,0:T(8,128)S(1)}) fusion(bf16[32,16,128,64]{2,3,1,0:T(8,128)(2,1)} %all-gather.21.cloned.1.call-done, f32[32,8]{1,0:T(8,128)S(1)} %exponential_select_fusion.1, f32[32,8]{1,0:T(8,128)S(1)} %get-tuple-element.212), kind=kLoop, calls=%fused_computation.7 | loop fusion | flops 12451840 | bytes 8914944 | tf_op jit(solution)/shard_map/reduce_sum | solution.py:275
  346.5 2.2 fusion.44
  349.9 2.6 fusion.36
  353.3 5.9 %rev.37 = f32[512,512]{0,1:T(8,128)} reverse(f32[512,512]{0,1:T(8,128)S(1)} %bitcast.319), dimensions={0} | reverse | bytes 2097152 | tf_op jit(solution)/shard_map/rev | solution.py:296
  359.2 2.8 fusion.46
  362.3 2.7 fusion.27
  368.5 2.6 convolution_convert_fusion
  371.0 6.0 %all-to-all-start = ((bf16[4,128,2048]{2,1,0:T(8,128)(2,1)}), bf16[4,128,2048]{2,1,0:T(8,128)(2,1)}, u32[]{:S(2)}, u32[]{:S(2)}) async-start(bf16[4,128,2048]{2,1,0:T(8,128)(2,1)} %bitcast.323), calls=%async_computation | async-start | bytes 4194304 | tf_op jit(solution)/shard_map/all_to_all | solution.py:38
  377.2 24.7 %all-gather = f32[16384]{0:T(1024)S(1)} all-gather(f32[2048]{0:T(1024)S(1)} %bitcast.353), channel_id=2, replica_groups=mesh['sp_0'=8,'sp_1'=4,'tp'=4,'dp'=2] {'sp_0'}, dimensions={0}, use_global_device_ids=true | all-gather | bytes 73728 | tf_op jit(solution)/shard_map/all_gather | solution.py:19
  402.0 11.9 %all-gather.1 = f32[8192]{0:T(1024)S(1)} all-gather(f32[2048]{0:T(1024)S(1)} %reduce.6), channel_id=3, replica_groups=mesh['sp_0'=8,'sp_1'=4,'tp'=4,'dp'=2] {'sp_1'}, dimensions={0}, use_global_device_ids=true | all-gather | bytes 40960 | tf_op jit(solution)/shard_map/all_gather | solution.py:19
  413.9 11.9 %all-gather.2 = f32[8192]{0:T(1024)S(1)} all-gather(f32[2048]{0:T(1024)S(1)} %reduce.7), channel_id=4, replica_groups=mesh['sp_0'=8,'sp_1'=4,'tp'=4,'dp'=2] {'tp'}, dimensions={0}, use_global_device_ids=true | all-gather | bytes 40960 | tf_op jit(solution)/shard_map/all_gather | solution.py:19
  425.9 2.0 reduce_sum.188
  (288 shorter events, 91.6 us)
Async XLA Ops:
  6.5 361.9 %copy-start = (bf16[512,2048]{1,0:T(8,128)(2,1)S(1)}, bf16[512,2048]{1,0:T(8,128)(2,1)}, u32[]{:S(2)}) copy-start(bf16[512,2048]{1,0:T(8,128)(2,1)} %param.41) | copy-start | bytes 6291460
  6.5 105.3 %copy-start.1 = (bf16[1,128,2048]{2,1,0:T(8,128)(2,1)S(1)}, bf16[1,128,2048]{2,1,0:T(8,128)(2,1)}, u32[]{:S(2)}) copy-start(bf16[1,128,2048]{2,1,0:T(8,128)(2,1)} %param.23) | copy-start | bytes 1572868
  6.5 137.6 %all-gather.19.cloned.1.call-start = ((), (), s32[]{:S(2)}) async-start(), calls=%async_computation.1 | async-start | bytes 2621440 | tf_op jit(solution)/shard_map/all_gather | solution.py:167
  6.5 107.0 %copy-start.16 = (bf16[1,32,2048]{2,1,0:T(8,128)(2,1)S(1)}, bf16[1,32,2048]{2,1,0:T(8,128)(2,1)}, u32[]{:S(2)}) copy-start(bf16[1,32,2048]{2,1,0:T(8,128)(2,1)} %param.25) | copy-start | bytes 393220
  7.5 54.7 %copy-start.48 = (bf16[2,16]{1,0:T(2,128)(2,1)}, bf16[2,16]{1,0:T(2,128)(2,1)S(1)}, u32[]{:S(2)}) copy-start(bf16[2,16]{1,0:T(2,128)(2,1)S(1)} %fusion.152) | copy-start | bytes 196
  36.7 77.2 %copy-start.40 = (bf16[2048,2,32]{0,2,1:T(8,128)(2,1)S(1)}, bf16[2048,2,32]{0,2,1:T(8,128)(2,1)}, u32[]{:S(2)}) copy-start(bf16[2048,2,32]{0,2,1:T(8,128)(2,1)} %param.34) | copy-start | bytes 786436
  113.4 120.0 %all-gather.23.cloned.1.call-start = ((), (), s32[]{:S(2)}) async-start(), calls=%async_computation.3 | async-start | bytes 1892352 | tf_op jit(solution)/shard_map/all_gather | solution.py:26
  113.9 4.8 %copy-start.59 = (f32[2,32]{1,0:T(2,128)S(1)}, f32[2,32]{1,0:T(2,128)}, u32[]{:S(2)}) copy-start(f32[2,32]{1,0:T(2,128)} %param.35) | copy-start | bytes 772
  118.5 223.4 %all-gather.21.cloned.1.call-start = ((), (), s32[]{:S(2)}) async-start(), calls=%async_computation.2 | async-start | bytes 8650752 | tf_op jit(solution)/shard_map/all_gather | solution.py:26
  119.8 45.3 %copy-start.50 = (f32[8]{0:T(128)}, f32[8]{0:T(128)S(1)}, u32[]{:S(2)}) copy-start(f32[8]{0:T(128)S(1)} %get-tuple-element.233) | copy-start | bytes 100
  121.6 26.1 %copy-start.30 = (f32[1,512]{1,0:T(1,128)}, f32[1,512]{1,0:T(1,128)S(1)}, u32[]{:S(2)}) copy-start(f32[1,512]{1,0:T(1,128)S(1)} %get-tuple-element.205) | copy-start | bytes 6148
  121.6 26.1 %copy-start.32 = (f32[1,512]{1,0:T(1,128)}, f32[1,512]{1,0:T(1,128)S(1)}, u32[]{:S(2)}) copy-start(f32[1,512]{1,0:T(1,128)S(1)} %get-tuple-element.206) | copy-start | bytes 6148
  121.6 26.1 %copy-start.34 = (f32[1,512]{1,0:T(1,128)}, f32[1,512]{1,0:T(1,128)S(1)}, u32[]{:S(2)}) copy-start(f32[1,512]{1,0:T(1,128)S(1)} %get-tuple-element.207) | copy-start | bytes 6148
  121.6 26.1 %copy-start.36 = (f32[1,512]{1,0:T(1,128)}, f32[1,512]{1,0:T(1,128)S(1)}, u32[]{:S(2)}) copy-start(f32[1,512]{1,0:T(1,128)S(1)} %get-tuple-element.208) | copy-start | bytes 6148
  121.6 26.1 %copy-start.38 = (f32[1,512]{1,0:T(1,128)}, f32[1,512]{1,0:T(1,128)S(1)}, u32[]{:S(2)}) copy-start(f32[1,512]{1,0:T(1,128)S(1)} %get-tuple-element.209) | copy-start | bytes 6148
  123.4 53.3 %copy-start.43 = (f32[1,256]{1,0:T(1,128)}, f32[1,256]{1,0:T(1,128)S(1)}, u32[]{:S(2)}) copy-start(f32[1,256]{1,0:T(1,128)S(1)} %get-tuple-element.216) | copy-start | bytes 3076
  123.4 53.3 %copy-start.44 = (f32[1,256]{1,0:T(1,128)}, f32[1,256]{1,0:T(1,128)S(1)}, u32[]{:S(2)}) copy-start(f32[1,256]{1,0:T(1,128)S(1)} %get-tuple-element.217) | copy-start | bytes 3076
  123.4 53.3 %copy-start.45 = (f32[1,256]{1,0:T(1,128)}, f32[1,256]{1,0:T(1,128)S(1)}, u32[]{:S(2)}) copy-start(f32[1,256]{1,0:T(1,128)S(1)} %get-tuple-element.218) | copy-start | bytes 3076
  123.4 53.3 %copy-start.46 = (f32[1,256]{1,0:T(1,128)}, f32[1,256]{1,0:T(1,128)S(1)}, u32[]{:S(2)}) copy-start(f32[1,256]{1,0:T(1,128)S(1)} %get-tuple-element.219) | copy-start | bytes 3076
  123.4 53.3 %copy-start.47 = (f32[1,256]{1,0:T(1,128)}, f32[1,256]{1,0:T(1,128)S(1)}, u32[]{:S(2)}) copy-start(f32[1,256]{1,0:T(1,128)S(1)} %get-tuple-element.220) | copy-start | bytes 3076
  165.1 5.7 %copy-start.21 = (f32[512,2,8]{0,2,1:T(8,128)}, f32[512,2,8]{0,2,1:T(8,128)S(1)}, u32[]{:S(2)}) copy-start(f32[512,2,8]{0,2,1:T(8,128)S(1)} %bitcast_convert_fusion.1) | copy-start | bytes 98308
  165.5 6.2 %copy-start.23 = (f32[512,8]{0,1:T(8,128)}, f32[512,8]{0,1:T(8,128)S(1)}, u32[]{:S(2)}) copy-start(f32[512,8]{0,1:T(8,128)S(1)} %rev.31) | copy-start | bytes 49156
  168.1 3.6 copy-start.5
  179.3 9.4 %copy-start.9 = (bf16[8,64,256]{2,1,0:T(8,128)(2,1)}, bf16[8,64,256]{2,1,0:T(8,128)(2,1)S(1)}, u32[]{:S(2)}) copy-start(bf16[8,64,256]{2,1,0:T(8,128)(2,1)S(1)} %multiply_convert_fusion.24) | copy-start | bytes 786436
  190.2 8.1 %slice-start.1 = ((f32[512,2,8]{0,2,1:T(8,128)}), f32[512,1,8]{0,2,1:T(8,128)S(1)}, s32[]{:S(2)}) async-start(f32[512,2,8]{0,2,1:T(8,128)} %copy-done.21), calls=%async_computation.5 | async-start | bytes 32768 | tf_op jit(solution)/shard_map/slice | solution.py:198
  203.7 8.4 %copy-start.6 = (bf16[4,128,2,128]{3,2,1,0:T(2,128)(2,1)}, bf16[4,128,2,128]{3,2,1,0:T(2,128)(2,1)S(1)}, u32[]{:S(2)}) copy-start(bf16[4,128,2,128]{3,2,1,0:T(2,128)(2,1)S(1)} %convert_element_type.235) | copy-start | bytes 786436
  212.1 5.2 %copy-start.14 = (bf16[4,128,2,4,64]{1,4,3,2,0:T(8,128)(2,1)}, bf16[4,128,2,4,64]{1,4,3,2,0:T(8,128)(2,1)S(1)}, u32[]{:S(2)}) copy-start(bf16[4,128,2,4,64]{1,4,3,2,0:T(8,128)(2,1)S(1)} %copy.284) | copy-start | bytes 1572868
  217.3 12.3 %copy-start.22 = (f32[1,16384]{1,0:T(1,128)S(1)}, f32[1,16384]{1,0:T(1,128)}, u32[]{:S(2)}) copy-start(f32[1,16384]{1,0:T(1,128)} %param.36) | copy-start | bytes 196612
  233.4 4.0 copy-start.51
  233.4 4.0 copy-start.58
  233.5 3.8 slice-start
  260.1 4.7 %copy-start.7 = (bf16[4,128,2,128]{3,2,1,0:T(2,128)(2,1)S(1)}, bf16[4,128,2,128]{3,2,1,0:T(2,128)(2,1)}, u32[]{:S(2)}) copy-start(bf16[4,128,2,128]{3,2,1,0:T(2,128)(2,1)} %copy-done.6) | copy-start | bytes 786436
  262.8 7.2 %copy-start.4 = (f32[4,128,2,4]{3,2,1,0:T(2,128)S(1)}, f32[4,128,2,4]{3,2,1,0:T(2,128)}, u32[]{:S(2)}) copy-start(f32[4,128,2,4]{3,2,1,0:T(2,128)} %copy-done.3) | copy-start | bytes 49156
  270.0 59.3 %copy-start.11 = (bf16[8,64,256]{2,1,0:T(8,128)(2,1)S(1)}, bf16[8,64,256]{2,1,0:T(8,128)(2,1)}, u32[]{:S(2)}) copy-start(bf16[8,64,256]{2,1,0:T(8,128)(2,1)} %copy-done.10) | copy-start | bytes 786436
  273.1 63.8 %copy-start.15 = (bf16[4,128,2,4,64]{1,4,3,2,0:T(8,128)(2,1)S(1)}, bf16[4,128,2,4,64]{1,4,3,2,0:T(8,128)(2,1)}, u32[]{:S(2)}) copy-start(bf16[4,128,2,4,64]{1,4,3,2,0:T(8,128)(2,1)} %copy-done.14) | copy-start | bytes 1572868
  273.1 63.8 %copy-start.25 = (f32[4,128,2,4]{1,3,2,0:T(4,128)S(1)}, f32[4,128,2,4]{1,3,2,0:T(4,128)}, u32[]{:S(2)}) copy-start(f32[4,128,2,4]{1,3,2,0:T(4,128)} %get-tuple-element.196) | copy-start | bytes 49156
  273.1 63.8 %copy-start.26 = (f32[4,128,2,4]{1,3,2,0:T(4,128)S(1)}, f32[4,128,2,4]{1,3,2,0:T(4,128)}, u32[]{:S(2)}) copy-start(f32[4,128,2,4]{1,3,2,0:T(4,128)} %copy.282) | copy-start | bytes 49156
  341.9 4.6 %copy-start.17 = (f32[1024,2,128]{2,0,1:T(8,128)S(1)}, f32[1024,2,128]{2,0,1:T(8,128)}, u32[]{:S(2)}) copy-start(f32[1024,2,128]{2,0,1:T(8,128)} %copy.301) | copy-start | bytes 3145732
  341.9 4.6 %copy-start.19 = (bf16[1,1024,512]{1,2,0:T(8,128)(2,1)S(1)}, bf16[1,1024,512]{1,2,0:T(8,128)(2,1)}, u32[]{:S(2)}) copy-start(bf16[1,1024,512]{1,2,0:T(8,128)(2,1)} %multiply_convert_fusion.5) | copy-start | bytes 3145732
  341.9 4.6 %copy-start.29 = (f32[1024,2,4]{0,2,1:T(4,128)S(1)}, f32[1024,2,4]{0,2,1:T(4,128)}, u32[]{:S(2)}) copy-start(f32[1024,2,4]{0,2,1:T(4,128)} %mul.818) | copy-start | bytes 98308
  341.9 4.6 %copy-start.61 = (f32[2,4]{1,0:T(2,128)S(1)}, f32[2,4]{1,0:T(2,128)}, u32[]{:S(2)}) copy-start(f32[2,4]{1,0:T(2,128)} %exp.182) | copy-start | bytes 100
  353.2 6.0 %copy-start.28 = (f32[1024,2,4]{0,2,1:T(4,128)S(1)}, f32[1024,2,4]{0,2,1:T(4,128)}, u32[]{:S(2)}) copy-start(f32[1024,2,4]{0,2,1:T(4,128)} %mul.787) | copy-start | bytes 98308
  362.3 3.5 copy-start.18
  362.3 3.5 copy-start.60
  371.0 6.0 %copy-start.27 = (bf16[16,2048]{1,0:T(8,128)(2,1)S(1)}, bf16[16,2048]{1,0:T(8,128)(2,1)}, u32[]{:S(2)}) copy-start(bf16[16,2048]{1,0:T(8,128)(2,1)} %param.29) | copy-start | bytes 196612
  371.0 6.0 %copy-start.49 = (bf16[2,16]{1,0:T(2,128)(2,1)S(1)}, bf16[2,16]{1,0:T(2,128)(2,1)}, u32[]{:S(2)}) copy-start(bf16[2,16]{1,0:T(2,128)(2,1)} %copy-done.48) | copy-start | bytes 196
  371.0 54.9 %all-to-all-start = ((bf16[4,128,2048]{2,1,0:T(8,128)(2,1)}), bf16[4,128,2048]{2,1,0:T(8,128)(2,1)}, u32[]{:S(2)}, u32[]{:S(2)}) async-start(bf16[4,128,2048]{2,1,0:T(8,128)(2,1)} %bitcast.323), calls=%async_computation | async-start | bytes 4194304 | tf_op jit(solution)/shard_map/all_to_all | solution.py:38
  377.1 50.9 %copy-start.2 = (bf16[1,128,2048]{2,1,0:T(8,128)(2,1)S(1)}, bf16[1,128,2048]{2,1,0:T(8,128)(2,1)}, u32[]{:S(2)}) copy-start(bf16[1,128,2048]{2,1,0:T(8,128)(2,1)} %param.23) | copy-start | bytes 1572868
  (20 other events, 40.9 us)
Sparse Core Ops, SparseCore 0:
  113.6 30.5 all-gather.18
  146.7 78.5 all-gather.22
  229.1 101.3 all-gather.20
